TPU v7x, 128 devices: a whole 4x4x4 slice. The times are simulated.
128 devices in a mesh: fs: 16 (over z, x), tp: 8 (over y, core).
Axes of the slice: x: 4, y: 4, z: 4, core: 2. Of those that a mesh axis runs over, the one named last changes fastest.
Arguments:
- mixer_input: bfloat16 [16384, 4096], P('fs'), may hold values from -6 to 6
- cell_output: bfloat16 [16384, 2048], P('fs'), may hold values from -6 to 6
- query_grad: bfloat16 [16384, 2048], P('fs', 'tp'), may hold values from -4 to 4
- value_grad: bfloat16 [16384, 2048], P('fs', 'tp'), may hold values from -4 to 4
- output_grad: bfloat16 [16384, 4096], P('fs', 'tp'), may hold values from -4 to 4
- query_weight: float32 [4096, 2048], P('fs', 'tp'), may hold values from -6 to 6
- value_weight: float32 [4096, 2048], P('fs', 'tp'), may hold values from -6 to 6
- output_weight: float32 [2048, 4096], P('fs', 'tp'), may hold values from -6 to 6
- query_basis: bfloat16 [4096, 128], P('fs'), may hold values from -0.09375 to 0.09375
- value_basis: bfloat16 [4096, 128], P('fs'), may hold values from -0.09375 to 0.09375
- output_basis: bfloat16 [2048, 128], P('fs'), may hold values from -0.125 to 0.125
- query_mean: float32 [128, 2048], P(None, 'tp'), may hold values from -6 to 6
- value_mean: float32 [128, 2048], P(None, 'tp'), may hold values from -6 to 6
- output_mean: float32 [128, 4096], P(None, 'tp'), may hold values from -6 to 6
- query_square: float32 [128, 2048], P(None, 'tp'), may hold values from 0.25 to 4
- value_square: float32 [128, 2048], P(None, 'tp'), may hold values from 0.25 to 4
- output_square: float32 [128, 4096], P(None, 'tp'), may hold values from 0.25 to 4
Outputs:
- query_step: float32 [4096, 2048], P('fs', 'tp')
- value_step: float32 [4096, 2048], P('fs', 'tp')
- output_step: float32 [2048, 4096], P('fs', 'tp')
- query_copy: bfloat16 [4096, 2048], P(None, 'tp')
- value_copy: bfloat16 [4096, 2048], P(None, 'tp')
- output_copy: bfloat16 [2048, 4096], P(None, 'tp')
- query_first: float32 [128, 2048], P(None, 'tp')
- value_first: float32 [128, 2048], P(None, 'tp')
- output_first: float32 [128, 4096], P(None, 'tp')
- query_second: float32 [128, 2048], P(None, 'tp')
- value_second: float32 [128, 2048], P(None, 'tp')
- output_second: float32 [128, 4096], P(None, 'tp')
All inputs are finite; a program needn't handle non-finite values.
Results may differ from a plain program's by a relative error of at most 0.013.
Values may be sent and summed in bfloat16 or wider, within the bound.
A program may use at most 128 MiB of HBM per device.

v0:
```python
import functools

import jax
import jax.numpy as jnp
from jax import lax
from jax.experimental import pallas as pl
from jax.experimental.pallas import tpu as pltpu
from jax.sharding import PartitionSpec as P

MODEL = 4096
CELL = 2048

beta_first = 0.8
beta_second = 0.9
floor_mean = 0.005
learn_rate = 0.05

f32 = jnp.float32
bf16 = jnp.bfloat16
HIGH = lax.Precision.HIGHEST
SIDE = 4
FS = SIDE * SIDE
TP = 8
B_ROWS = 320
W_ROWS = 384
COLS = 64
SLICE = B_ROWS // TP
W_CUTS = ((0, 96), (96, 96), (192, 96), (288, 96))
NEAR = [(0, 1), (0, -1), (1, 0), (-1, 0)]
ACROSS = [(0, 2), (2, 0)]
DIAGONAL = [(-1, -1), (-1, 1), (1, -1), (1, 1)]
FAR = [(-1, 2), (2, -1), (1, 2), (2, 1), (2, 2)]
GROUPS = (NEAR, ACROSS, DIAGONAL, FAR)
OTHERS = NEAR + ACROSS + DIAGONAL + FAR
MESH = pl.DeviceIdType.MESH


def slot(dz, dx):
    return (dz % SIDE) * SIDE + dx % SIDE


def link_plan(along_x, sign):
    near, far = ((0, 1), (2, 3)) if along_x else ((2, 3), (0, 1))
    which = 0 if sign > 0 else 1

    def at(far_off, near_off):
        return (far_off, near_off) if along_x else (near_off, far_off)

    steps = [(at(0, 0), near[0]), (at(0, 0), near[1]), (at(0, 0), far[0]), (at(0, 0), far[1])]
    steps.append((at(0, -sign), near[which]))
    steps += [(at(-1, 0), far[0]), (at(-1, 0), far[1]), (at(1, 0), far[0]), (at(1, 0), far[1])]
    steps.append((at(0, -sign), far[which]))
    steps += [(at(2, 0), far[0]), (at(2, 0), far[1])]
    steps += [(at(-1, -sign), far[which]), (at(1, -sign), far[which]), (at(2, -sign), far[which])]
    return steps


LINKS = [(True, 1), (True, -1), (False, 1), (False, -1)]
PLANS = [link_plan(*link) for link in LINKS]
STEPS = 15


def dot00(a, b):
    return lax.dot_general(a, b, (((0,), (0,)), ((), ())), preferred_element_type=f32)


def dot(a, b):
    return jnp.dot(a, b, preferred_element_type=f32)


def arrivals():
    got = {}
    for (along_x, sign), plan in zip(LINKS, PLANS):
        for s, (off, piece) in enumerate(plan):
            dest = (off[0], off[1] - sign) if along_x else (off[0] - sign, off[1])
            got[slot(*dest), piece] = s
    return got


ARRIVALS = arrivals()


class Torus:
    def __init__(self, buf, rows, send, recv, blk, neighbour):
        self.buf, self.rows, self.send, self.recv = buf, rows, send, recv
        self.blk, self.neighbour = blk, neighbour
        self.seen = set()

    def copy(self, src, dst, send, recv, link):
        return pltpu.make_async_remote_copy(
            src_ref=src,
            dst_ref=dst,
            send_sem=send,
            recv_sem=recv,
            device_id={"fs": self.neighbour[link]},
            device_id_type=MESH,
        )

    def need(self, off, piece):
        s = ARRIVALS.get((slot(*off), piece))
        if s is None or s in self.seen:
            return
        self.seen.add(s)
        block = self.buf.at[0]
        self.copy(block, block, self.send, self.recv.at[s], 0).wait_recv()

    def step(self, s):
        for link in range(len(LINKS)):
            off, piece = PLANS[link][s]
            self.need(off, piece)
            start, size = self.rows[piece]
            ref = self.buf.at[self.blk(*off), pl.ds(start, size), :]
            self.copy(ref, ref, self.send, self.recv.at[s], link).start()

    def block(self, off):
        for piece in range(4):
            self.need(off, piece)

    def finish(self):
        sent = self.buf.at[pl.ds(0, STEPS)]
        self.copy(sent, sent, self.send, self.recv.at[0], 0).wait_send()


def gather_kernel(
    x_h, c_h, gq_h, gv_h, go_h, wq_h, wv_h, wo_h, bq_h, bv_h, bo_h,
    mq_h, mv_h, mo_h, sq_h, sv_h, so_h,
    wall, ball, dcopy, stq, stv, sto, f1q, f1v, f1o, f2q, f2v, f2o,
    x, c, gq, gv, go, wqv, wo, mean, square,
    xb, cb, gt, hl, psend, precv, pall, gram, turned, d, sqf, sqs,
    lsem, wsend, wrecv, bsend, brecv, psems, psemr, ysend, yrecv, rsend, rrecv, asend, arecv,
    fsend, frecv, ssend, srecv,
):
    f = lax.axis_index("fs")
    t = lax.axis_index("tp")
    z, xx = f // SIDE, lax.rem(f, SIDE)
    core = lax.rem(t, 2)

    def blk(dz, dx):
        return lax.rem(z + (dz % SIDE), SIDE) * SIDE + lax.rem(xx + (dx % SIDE), SIDE)

    def load(src, dst, sem):
        pltpu.make_async_copy(src, dst, lsem.at[sem]).start()

    def loaded(ref, sem):
        pltpu.make_async_copy(ref, ref, lsem.at[sem]).wait()

    load(bq_h, ball.at[f, pl.ds(0, 256), pl.ds(0, 128)], 0)
    load(bv_h, ball.at[f, pl.ds(0, 256), pl.ds(128, 128)], 0)
    load(bo_h.at[pl.ds(0, 64), :], ball.at[f, pl.ds(256, 64), pl.ds(0, 128)], 0)
    load(bo_h.at[pl.ds(64, 64), :], ball.at[f, pl.ds(256, 64), pl.ds(128, 128)], 0)
    load(wq_h, wqv.at[:, pl.ds(0, 256)], 1)
    load(wv_h, wqv.at[:, pl.ds(256, 256)], 1)
    load(wo_h, wo, 2)
    load(x_h, x, 3)
    load(c_h, c, 4)
    load(gq_h, gq, 5)
    load(gv_h, gv, 6)
    load(go_h, go, 7)
    for at, mean_in, square_in in ((0, mq_h, sq_h), (256, mv_h, sv_h), (512, mo_h, so_h)):
        cols = pl.ds(at, mean_in.shape[1])
        load(mean_in, mean.at[:, cols], 8)
        load(square_in, square.at[:, cols], 9)

    barrier = pltpu.get_barrier_semaphore()
    for off in OTHERS:
        pl.semaphore_signal(barrier, inc=1, device_id={"fs": blk(*off)}, device_id_type=MESH)
    for r in range(1, TP):
        pl.semaphore_signal(
            barrier, inc=1, device_id={"tp": lax.rem(t + r, TP)}, device_id_type=MESH
        )
    loaded(ball.at[f], 0)
    pl.semaphore_wait(barrier, FS - 1 + TP - 1)

    neighbour = [blk(0, 1), blk(0, -1), blk(1, 0), blk(-1, 0)]
    weights = Torus(wall, W_CUTS, wsend, wrecv, blk, neighbour)
    y = t // 2
    above, below = lax.rem(y + 1, SIDE), lax.rem(y + SIDE - 1, SIDE)
    groups = GROUPS

    def slice_rows(level, start, size):
        return pl.ds(pl.multiple_of((core * SIDE + level) * SLICE + start, 8), size)

    def remote(src, dst, send, recv, device_id):
        return pltpu.make_async_remote_copy(
            src_ref=src,
            dst_ref=dst,
            send_sem=send,
            recv_sem=recv,
            device_id=device_id,
            device_id_type=MESH,
        )

    def received(ref, recv):
        remote(ref, ref, recv, recv, {"fs": neighbour[0]}).wait_recv()

    def sent(ref, send):
        remote(ref, ref, send, send, {"fs": neighbour[0]}).wait_send()

    def group_of(off):
        return [slot(*off) in [slot(*o) for o in g] for g in groups].index(True)

    def in_plane(off, start, size, to):
        arriving = (off[0] - to[0], off[1] - to[1])
        ref = ball.at[blk(*off), slice_rows(y, start, size), :]
        remote(ref, ref, bsend, brecv.at[group_of(arriving)], {"fs": blk(*to)}).start()

    def x_first(off):
        return 24 if (off[0] + off[1]) % 2 else 16

    def turn(blocks):
        for dz, dx in blocks:
            peers = [(1, 0), (-1, 0), (2, 0)] if dz == 0 else [(0, 1), (0, -1), (0, 2)]
            for to in peers:
                h = x_first((dz - to[0], dx - to[1]))
                in_plane((dz, dx), *((0, h) if dz == 0 else (h, SLICE - h)), to)

    def level(off, rows, up, recv):
        ref = ball.at[blk(*off), slice_rows(*rows), :]
        remote(ref, ref, ysend, recv, {"tp": (above if up else below) * 2 + core}).start()

    def send_levels(i):
        received(ball.at[pl.ds(0, len(groups[i])), pl.ds(0, SLICE), :], brecv.at[i])
        for off in groups[i]:
            level(off, (y, 0, SLICE), True, yrecv.at[i])
            level(off, (y, 0, SLICE), False, yrecv.at[i])

    def relay_levels(i):
        received(ball.at[pl.ds(0, len(groups[i])), pl.ds(0, 2 * SLICE), :], yrecv.at[i])
        for off in groups[i]:
            half = 24 if OTHERS.index(off) % 2 else 16
            level(off, (below, 0, half), True, yrecv.at[len(GROUPS) + i])
            level(off, (above, half, SLICE - half), False, yrecv.at[len(GROUPS) + i])

    def hand_over(i):
        received(ball.at[pl.ds(0, len(groups[i])), pl.ds(0, SLICE), :], yrecv.at[len(GROUPS) + i])
        rows = pl.ds(pl.multiple_of(core * SIDE * SLICE, 8), SIDE * SLICE)
        for off in groups[i]:
            ref = ball.at[blk(*off), rows, :]
            remote(ref, ref, psems, psemr.at[i], {"tp": t + 1 - 2 * core}).start()

    def handed(i):
        received(ball.at[pl.ds(0, len(groups[i])), pl.ds(0, SIDE * SLICE), :], psemr.at[i])

    def outputs_of(b):
        return jnp.concatenate([ball[b, 256:320, 0:128], ball[b, 256:320, 128:256]], axis=0)

    def project(offs, first=False):
        bs = [blk(*off) for off in offs]
        xs = [x[:, pl.ds(pl.multiple_of(b * 256, 256), 256)] for b in bs]
        cs = [c[:, pl.ds(pl.multiple_of(b * 128, 128), 128)] for b in bs]
        px = dot(
            jnp.concatenate(xs, axis=1), jnp.concatenate([ball[b, 0:256, :] for b in bs], axis=0)
        )
        pc = dot(jnp.concatenate(cs, axis=1), jnp.concatenate([outputs_of(b) for b in bs], axis=0))
        if first:
            xb[...] = px
            cb[...] = pc
        else:
            xb[...] += px
            cb[...] += pc

    for off in NEAR + ACROSS:
        in_plane((0, 0), 0, SLICE, off)
    loaded(wqv, 1)
    loaded(wo, 2)
    wall[f, 0:256, :] = wqv[...].astype(bf16)
    wall[f, 256:384, :] = wo[...].astype(bf16)
    weights.step(0)
    send_levels(0)
    turn(NEAR)
    send_levels(1)
    turn(ACROSS)
    for s in range(1, 4):
        weights.step(s)
    loaded(x, 3)
    loaded(c, 4)
    project([(0, 0)], first=True)
    relay_levels(0)
    send_levels(2)
    for g, sem, lo, hi in ((gq, 5, 0, 256), (gv, 6, 256, 512), (go, 7, 512, 1024)):
        loaded(g, sem)
        gt[lo:hi, :] = g[...].T
    relay_levels(1)
    send_levels(3)
    weights.step(4)
    hand_over(0)
    relay_levels(2)
    hand_over(1)
    weights.step(5)
    relay_levels(3)
    weights.step(6)
    handed(0)
    project(NEAR[0:2])
    project(NEAR[2:4])
    hand_over(2)
    weights.step(7)
    handed(1)
    project(ACROSS)
    hand_over(3)
    weights.step(8)
    handed(2)
    project(DIAGONAL[0:2])
    project(DIAGONAL[2:4])
    weights.step(9)
    handed(3)
    project(FAR[0:2])
    project(FAR[2:4])
    project(FAR[4:5])


    def split(a, at):
        hi = a.astype(bf16)
        hl[:, at : at + 128] = hi
        hl[:, at + 128 : at + 256] = (a - hi.astype(f32)).astype(bf16)

    split(xb[:, 0:128], 0)
    split(xb[:, 128:256], 256)
    split(cb[...], 512)
    for at, lo, hi in ((0, 0, 256), (256, 256, 512), (512, 512, 1024)):
        both = dot(gt[lo:hi, :], hl[:, at : at + 256])
        both = (both[:, 0:128] + both[:, 128:256]).astype(bf16)
        for j in range(lo // COLS, hi // COLS):
            psend[j] = both[j * COLS - lo : (j + 1) * COLS - lo, :]

    def grams(js, first=False):
        gq_sum = jnp.zeros((256, 256), f32)
        go_sum = jnp.zeros((128, 128), f32)
        for j in js:
            bqv = ball[j, 0:256, :]
            bo = outputs_of(j)
            gq_sum += dot00(bqv, bqv)
            go_sum += dot00(bo, bo)
        for i, g in enumerate((gq_sum[0:128, 0:128], gq_sum[128:256, 128:256], go_sum)):
            gram[i] = g if first else gram[i] + g

    grams(range(0, 1), first=True)

    def to_peer(src, dst, send, recv, off):
        remote(src, dst, send, recv, {"fs": blk(*off)}).start()

    for off in OTHERS:
        to_peer(psend.at[blk(*off)], precv.at[f], rsend, rrecv, off)
    weights.step(10)
    grams(range(1, FS))
    precv[f] = psend[f]
    loaded(mean, 8)
    loaded(square, 9)
    slab = pl.ds(pl.multiple_of((f // 2) * 128, 128), 128)
    turned[0] = mean[:, slab].T
    turned[1] = square[:, slab].T
    weights.step(11)
    peers = pl.ds(0, FS - 1)
    received(precv.at[peers], rrecv)
    total = precv[0].astype(f32)
    for j in range(1, FS):
        total += precv[j].astype(f32)
    total = total.astype(bf16)
    pall[f] = total

    def moments(p, mean_old, square_old):
        one = beta_first * mean_old + (1.0 - beta_first) * p
        two = beta_second * square_old + (1.0 - beta_second) * p * p
        return one, two, one / jnp.sqrt(two)

    own = pl.ds(pl.multiple_of(lax.rem(f, 2) * COLS, COLS), COLS)
    _, _, own_d = moments(total.astype(f32), turned[0, own, :], turned[1, own, :])
    gd = jnp.dot(
        own_d, gram[jnp.minimum(f // 4, 2)], precision=HIGH, preferred_element_type=f32
    )
    sqf[f] = jnp.broadcast_to(jnp.sum(own_d * gd, keepdims=True), (1, 128))
    for off in OTHERS:
        to_peer(sqf.at[f], sqf.at[f], fsend, frecv, off)
    for off in NEAR + ACROSS:
        to_peer(pall.at[f], pall.at[f], asend, arecv.at[0], off)
    weights.step(12)
    weights.step(13)
    received(sqf.at[peers], frecv)
    squares = sqf[0]
    for j in range(1, FS):
        squares += sqf[j]
    sqs[t] = squares

    for r in range(1, TP):
        remote(sqs.at[t], sqs.at[t], ssend, srecv, {"tp": lax.rem(t + r, TP)}).start()
    received(pall.at[pl.ds(0, len(NEAR + ACROSS))], arecv.at[0])
    upper, lower = pl.ds(0, COLS // 2), pl.ds(COLS // 2, COLS // 2)
    for step in (1, -1, 2):
        for to in (1, -1, 2):
            ref = pall.at[blk(0, step), upper, :]
            to_peer(ref, ref, asend, arecv.at[1], (to, 0))
            ref = pall.at[blk(step, 0), lower, :]
            to_peer(ref, ref, asend, arecv.at[1], (0, to))
    weights.step(14)
    received(pall.at[pl.ds(0, len(DIAGONAL + FAR))], arecv.at[1])
    firsts = [(f1q, 0), (f1q, 128), (f1v, 0), (f1v, 128)] + [(f1o, 128 * i) for i in range(4)]
    seconds = [(f2q, 0), (f2q, 128), (f2v, 0), (f2v, 128)] + [(f2o, 128 * i) for i in range(4)]
    for k in range(8):
        at = slice(128 * k, 128 * k + 128)
        p = jnp.concatenate([pall[2 * k], pall[2 * k + 1]], axis=0).astype(f32).T
        one, two, d[:, at] = moments(p, mean[:, at], square[:, at])
        ref, lo = firsts[k]
        ref[:, lo : lo + 128] = one
        ref, lo = seconds[k]
        ref[:, lo : lo + 128] = two
    hi = d[...].astype(bf16)
    lo = (d[...] - hi.astype(f32)).astype(bf16)
    bqv, bo = ball[f, 0:256, :], outputs_of(f)
    low_q = dot(bqv[:, 0:128], hi[:, 0:256]) + dot(bqv[:, 0:128], lo[:, 0:256])
    low_v = dot(bqv[:, 128:256], hi[:, 256:512]) + dot(bqv[:, 128:256], lo[:, 256:512])
    low_o = dot(bo, hi[:, 512:1024]) + dot(bo, lo[:, 512:1024])
    stq[...] = low_q
    stv[...] = low_v
    sto[...] = low_o
    received(sqs.at[pl.ds(0, TP - 1)], srecv)
    squares = sqs[0]
    for i in range(1, TP):
        squares += sqs[i]
    factor = 1.0 / jnp.sqrt(squares[0:1, 0:1] / (3.0 * MODEL * CELL) + floor_mean)
    dcopy[...] = (-learn_rate * factor * d[...]).astype(bf16)
    stq[...] = -factor * stq[...]
    stv[...] = -factor * stv[...]
    sto[...] = -factor * sto[...]
    for off in OTHERS:
        weights.block(off)
    weights.finish()
    blocks = pl.ds(0, FS - 1)
    sent(ball.at[pl.ds(0, len(NEAR + ACROSS)), pl.ds(0, SLICE), :], bsend)
    sent(ball.at[pl.ds(0, len(DIAGONAL + FAR)), pl.ds(0, SLICE), :], bsend)
    sent(ball.at[blocks, pl.ds(0, 3 * SLICE), :], ysend)
    sent(ball.at[blocks, pl.ds(0, SIDE * SLICE), :], psems)
    sent(psend.at[peers], rsend)
    sent(pall.at[peers], asend)
    sent(sqf.at[peers], fsend)
    sent(sqs.at[pl.ds(0, TP - 1)], ssend)


def finish_kernel(
    wall, ball, dcopy, stq, stv, sto, f1q, f1v, f1o, f2q, f2v, f2o,
    o_stq, o_stv, o_sto, o_q, o_v, o_o, o_f1q, o_f1v, o_f1o, o_f2q, o_f2v, o_f2o,
    cq, cv, co, sem, csem,
):
    plain = [
        pltpu.make_async_copy(src, dst, sem.at[i])
        for i, (src, dst) in enumerate(
            (
                (stq, o_stq), (stv, o_stv), (sto, o_sto), (f1q, o_f1q), (f1v, o_f1v),
                (f1o, o_f1o), (f2q, o_f2q), (f2v, o_f2v), (f2o, o_f2o),
            )
        )
    ]
    for cp in plain:
        cp.start()
    for k in range(FS):
        bo = jnp.concatenate([ball[k, 256:320, 0:128], ball[k, 256:320, 128:256]], axis=0)
        wq = wall[k, 0:256, 0:256].astype(f32)
        cq[k * 256 : k * 256 + 256, :] = (
            wq + dot(ball[k, 0:256, 0:128], dcopy[:, 0:256])
        ).astype(bf16)
        wv = wall[k, 0:256, 256:512].astype(f32)
        cv[k * 256 : k * 256 + 256, :] = (
            wv + dot(ball[k, 0:256, 128:256], dcopy[:, 256:512])
        ).astype(bf16)
        wo = wall[k, 256:384, :].astype(f32)
        co[k * 128 : k * 128 + 128, :] = (wo + dot(bo, dcopy[:, 512:1024])).astype(bf16)
        for i, (src, dst, n) in enumerate(((cq, o_q, 256), (cv, o_v, 256), (co, o_o, 128))):
            cp = pltpu.make_async_copy(
                src.at[pl.ds(k * n, n), :], dst.at[pl.ds(k * n, n), :], csem.at[i]
            )
            cp.start()
    for cp in plain:
        cp.wait()
    for i, (src, dst) in enumerate(((cq, o_q), (cv, o_v), (co, o_o))):
        pltpu.make_async_copy(src, dst, csem.at[i]).wait()


def local(*args):
    tokens = args[0].shape[0]
    any_spec = pl.BlockSpec(memory_space=pl.ANY)
    vmem_spec = pl.BlockSpec(memory_space=pltpu.VMEM)
    steps = [((256, 256), f32), ((256, 256), f32), ((128, 512), f32)]
    news = [((MODEL, 256), bf16), ((MODEL, 256), bf16), ((CELL, 512), bf16)]
    moment = [((128, 256), f32), ((128, 256), f32), ((128, 512), f32)]
    mids = [((FS, W_ROWS, 512), bf16), ((FS, B_ROWS, 256), bf16), ((128, 1024), bf16)]
    mids += steps + moment + moment
    outs = steps + news + moment + moment
    dma = pltpu.SemaphoreType.DMA
    mid = pl.pallas_call(
        gather_kernel,
        out_shape=[pltpu.VMEM(s, t) for s, t in mids],
        in_specs=[any_spec] * 17,
        out_specs=[vmem_spec] * len(mids),
        scratch_shapes=[
            pltpu.VMEM((tokens, MODEL), bf16),
            pltpu.VMEM((tokens, CELL), bf16),
            pltpu.VMEM((tokens, 256), bf16),
            pltpu.VMEM((tokens, 256), bf16),
            pltpu.VMEM((tokens, 512), bf16),
            pltpu.VMEM((256, 512), f32),
            pltpu.VMEM((128, 512), f32),
            pltpu.VMEM((128, 1024), f32),
            pltpu.VMEM((128, 1024), f32),
            pltpu.VMEM((tokens, 256), f32),
            pltpu.VMEM((tokens, 128), f32),
            pltpu.VMEM((1024, tokens), bf16),
            pltpu.VMEM((tokens, 768), bf16),
            pltpu.VMEM((FS, COLS, 128), bf16),
            pltpu.VMEM((FS, COLS, 128), bf16),
            pltpu.VMEM((FS, COLS, 128), bf16),
            pltpu.VMEM((3, 128, 128), f32),
            pltpu.VMEM((2, 128, 128), f32),
            pltpu.VMEM((128, 1024), f32),
            pltpu.VMEM((FS, 1, 128), f32),
            pltpu.VMEM((TP, 1, 128), f32),
            dma((10,)),
            dma, dma((STEPS,)), dma, dma((4,)), dma, dma((4,)), dma, dma((8,)),
            dma, dma, dma, dma((2,)), dma, dma, dma, dma,
        ],
        compiler_params=pltpu.CompilerParams(
            collective_id=0, has_side_effects=True, vmem_limit_bytes=50 * 1024 * 1024
        ),
        name="gather_and_reduce",
    )(*args)
    return tuple(
        pl.pallas_call(
            finish_kernel,
            out_shape=[jax.ShapeDtypeStruct(s, t) for s, t in outs],
            in_specs=[vmem_spec] * len(mids),
            out_specs=[any_spec] * len(outs),
            scratch_shapes=[
                pltpu.VMEM((MODEL, 256), bf16),
                pltpu.VMEM((MODEL, 256), bf16),
                pltpu.VMEM((CELL, 512), bf16),
                dma((9,)),
                dma((3,)),
            ],
            compiler_params=pltpu.CompilerParams(vmem_limit_bytes=12 * 1024 * 1024),
            name="write_copies",
        )(*mid)
    )


def solution(mesh):
    fs, both, tp = P("fs", None), P("fs", "tp"), P(None, "tp")
    in_specs = (fs, fs) + (both,) * 6 + (fs,) * 3 + (tp,) * 6
    out_specs = (both,) * 3 + (tp,) * 9
    return jax.shard_map(local, mesh=mesh, in_specs=in_specs, out_specs=out_specs, check_vma=False)
```

profile of v0, /device:TPU:0, one launch (start us, length us, event | category | flops | bytes accessed | tf_op | source)
XLA Modules:
  0.0 53.0 jit_solution(10073017170085894885)
XLA Ops:
  0.7 48.8 %gather_and_reduce.1 = (bf16[16,384,512]{2,1,0:T(8,128)(2,1)S(1)}, bf16[16,320,256]{2,1,0:T(8,128)(2,1)S(1)}, bf16[128,1024]{1,0:T(8,128)(2,1)S(1)}, f32[256,256...) custom-call(bf16[1024,4096]{1,0:T(8,128)(2,1)} %x_h.1, ...), custom_call_target="tpu_custom_call" | custom-call | tf_op jit(solution)/shard_map/gather_and_reduce/pallas_call | solution.py:487
  49.5 3.5 %write_copies.1 = (f32[256,256]{1,0:T(8,128)}, f32[256,256]{1,0:T(8,128)}, f32[128,512]{1,0:T(8,128)}, bf16[4096,256]{1,0:T(8,128)(2,1)}, bf16[4096,256]{1,0:T(8...) custom-call(bf16[16,384,512]{2,1,0:T(8,128)(2,1)S(1)} %get-tuple-ele, ...), custom_call_target="tpu_custom_call" | custom-call | tf_op jit(solution)/shard_map/write_copies/pallas_call | solution.py:524
where the time goes:
time: 53.4 us; the launch traced here: 53 us
  Pallas kernels  52.3 us (98%)
  between operations  0.66 us (1%)
    pallas_call x1, Pallas kernels, local(): pl.pallas_call(gather_kernel, out_shape=[pltpu.VMEM(s, t) for s, t in mid...  48.8 us
    pallas_call x1, Pallas kernels, local(): pl.pallas_call(finish_kernel, out_shape=[jax.ShapeDtypeStruct(s, t) for s...  3.49 us

commit v1 on v0

--- a/solution.py
+++ b/solution.py
@@ -24,7 +24,7 @@
 B_ROWS = 320
 W_ROWS = 384
 COLS = 64
-SLICE = B_ROWS // TP
+SLICES = (32, 48)
 W_CUTS = ((0, 96), (96, 96), (192, 96), (288, 96))
 NEAR = [(0, 1), (0, -1), (1, 0), (-1, 0)]
 ACROSS = [(0, 2), (2, 0)]
@@ -177,8 +177,13 @@
     above, below = lax.rem(y + 1, SIDE), lax.rem(y + SIDE - 1, SIDE)
     groups = GROUPS
 
-    def slice_rows(level, start, size):
-        return pl.ds(pl.multiple_of((core * SIDE + level) * SLICE + start, 8), size)
+    def by_core(fn):
+        for own in range(2):
+            pl.when(core == own)(functools.partial(fn, own, SLICES[own]))
+
+    def slice_rows(own, level, start, size):
+        at = own * SIDE * SLICES[0] + level * SLICES[own] + start
+        return pl.ds(pl.multiple_of(at, 8), size)
 
     def remote(src, dst, send, recv, device_id):
         return pltpu.make_async_remote_copy(
@@ -199,47 +204,55 @@
     def group_of(off):
         return [slot(*off) in [slot(*o) for o in g] for g in groups].index(True)
 
-    def in_plane(off, start, size, to):
+    def in_plane(own, off, start, size, to):
         arriving = (off[0] - to[0], off[1] - to[1])
-        ref = ball.at[blk(*off), slice_rows(y, start, size), :]
+        ref = ball.at[blk(*off), slice_rows(own, y, start, size), :]
         remote(ref, ref, bsend, brecv.at[group_of(arriving)], {"fs": blk(*to)}).start()
 
-    def x_first(off):
-        return 24 if (off[0] + off[1]) % 2 else 16
-
-    def turn(blocks):
+    def spread_own(own, size):
+        for off in NEAR + ACROSS:
+            in_plane(own, (0, 0), 0, size, off)
+
+    def turn(blocks, own, size):
         for dz, dx in blocks:
             peers = [(1, 0), (-1, 0), (2, 0)] if dz == 0 else [(0, 1), (0, -1), (0, 2)]
             for to in peers:
-                h = x_first((dz - to[0], dx - to[1]))
-                in_plane((dz, dx), *((0, h) if dz == 0 else (h, SLICE - h)), to)
-
-    def level(off, rows, up, recv):
-        ref = ball.at[blk(*off), slice_rows(*rows), :]
+                in_plane(own, (dz, dx), 0 if dz == 0 else size // 2, size // 2, to)
+
+    def level(own, off, rows, up, recv):
+        ref = ball.at[blk(*off), slice_rows(own, *rows), :]
         remote(ref, ref, ysend, recv, {"tp": (above if up else below) * 2 + core}).start()
 
-    def send_levels(i):
-        received(ball.at[pl.ds(0, len(groups[i])), pl.ds(0, SLICE), :], brecv.at[i])
+    def send_levels(i, own, size):
+        received(ball.at[pl.ds(0, len(groups[i])), pl.ds(0, size), :], brecv.at[i])
         for off in groups[i]:
-            level(off, (y, 0, SLICE), True, yrecv.at[i])
-            level(off, (y, 0, SLICE), False, yrecv.at[i])
-
-    def relay_levels(i):
-        received(ball.at[pl.ds(0, len(groups[i])), pl.ds(0, 2 * SLICE), :], yrecv.at[i])
+            level(own, off, (y, 0, size), True, yrecv.at[i])
+            level(own, off, (y, 0, size), False, yrecv.at[i])
+        if i < 2:
+            turn(groups[i], own, size)
+
+    def relay_levels(i, own, size):
+        received(ball.at[pl.ds(0, len(groups[i])), pl.ds(0, 2 * size), :], yrecv.at[i])
         for off in groups[i]:
-            half = 24 if OTHERS.index(off) % 2 else 16
-            level(off, (below, 0, half), True, yrecv.at[len(GROUPS) + i])
-            level(off, (above, half, SLICE - half), False, yrecv.at[len(GROUPS) + i])
-
-    def hand_over(i):
-        received(ball.at[pl.ds(0, len(groups[i])), pl.ds(0, SLICE), :], yrecv.at[len(GROUPS) + i])
-        rows = pl.ds(pl.multiple_of(core * SIDE * SLICE, 8), SIDE * SLICE)
+            recv = yrecv.at[len(GROUPS) + i]
+            level(own, off, (below, 0, size // 2), True, recv)
+            level(own, off, (above, size // 2, size // 2), False, recv)
+
+    def hand_over(i, own, size):
+        received(ball.at[pl.ds(0, len(groups[i])), pl.ds(0, size), :], yrecv.at[len(GROUPS) + i])
         for off in groups[i]:
-            ref = ball.at[blk(*off), rows, :]
-            remote(ref, ref, psems, psemr.at[i], {"tp": t + 1 - 2 * core}).start()
-
-    def handed(i):
-        received(ball.at[pl.ds(0, len(groups[i])), pl.ds(0, SIDE * SLICE), :], psemr.at[i])
+            ref = ball.at[blk(*off), pl.ds(own * SIDE * SLICES[0], SIDE * size), :]
+            remote(ref, ref, psems, psemr.at[i], {"tp": t + 1 - 2 * own}).start()
+
+    def handed(i, own, size):
+        rows = SIDE * SLICES[1 - own]
+        received(ball.at[pl.ds(0, len(groups[i])), pl.ds(0, rows), :], psemr.at[i])
+
+    def all_sent(own, size):
+        sent(ball.at[pl.ds(0, len(NEAR + ACROSS)), pl.ds(0, size), :], bsend)
+        sent(ball.at[pl.ds(0, len(DIAGONAL + FAR)), pl.ds(0, size), :], bsend)
+        sent(ball.at[pl.ds(0, FS - 1), pl.ds(0, 3 * size), :], ysend)
+        sent(ball.at[pl.ds(0, FS - 1), pl.ds(0, SIDE * size), :], psems)
 
     def outputs_of(b):
         return jnp.concatenate([ball[b, 256:320, 0:128], ball[b, 256:320, 128:256]], axis=0)
@@ -259,50 +272,47 @@
             xb[...] += px
             cb[...] += pc
 
-    for off in NEAR + ACROSS:
-        in_plane((0, 0), 0, SLICE, off)
+    by_core(spread_own)
     loaded(wqv, 1)
     loaded(wo, 2)
     wall[f, 0:256, :] = wqv[...].astype(bf16)
     wall[f, 256:384, :] = wo[...].astype(bf16)
     weights.step(0)
-    send_levels(0)
-    turn(NEAR)
-    send_levels(1)
-    turn(ACROSS)
+    by_core(functools.partial(send_levels, 0))
+    by_core(functools.partial(send_levels, 1))
     for s in range(1, 4):
         weights.step(s)
     loaded(x, 3)
     loaded(c, 4)
     project([(0, 0)], first=True)
-    relay_levels(0)
-    send_levels(2)
+    by_core(functools.partial(relay_levels, 0))
+    by_core(functools.partial(send_levels, 2))
     for g, sem, lo, hi in ((gq, 5, 0, 256), (gv, 6, 256, 512), (go, 7, 512, 1024)):
         loaded(g, sem)
         gt[lo:hi, :] = g[...].T
-    relay_levels(1)
-    send_levels(3)
+    by_core(functools.partial(relay_levels, 1))
+    by_core(functools.partial(send_levels, 3))
     weights.step(4)
-    hand_over(0)
-    relay_levels(2)
-    hand_over(1)
+    by_core(functools.partial(hand_over, 0))
+    by_core(functools.partial(relay_levels, 2))
+    by_core(functools.partial(hand_over, 1))
     weights.step(5)
-    relay_levels(3)
+    by_core(functools.partial(relay_levels, 3))
     weights.step(6)
-    handed(0)
+    by_core(functools.partial(handed, 0))
     project(NEAR[0:2])
     project(NEAR[2:4])
-    hand_over(2)
+    by_core(functools.partial(hand_over, 2))
     weights.step(7)
-    handed(1)
+    by_core(functools.partial(handed, 1))
     project(ACROSS)
-    hand_over(3)
+    by_core(functools.partial(hand_over, 3))
     weights.step(8)
-    handed(2)
+    by_core(functools.partial(handed, 2))
     project(DIAGONAL[0:2])
     project(DIAGONAL[2:4])
     weights.step(9)
-    handed(3)
+    by_core(functools.partial(handed, 3))
     project(FAR[0:2])
     project(FAR[2:4])
     project(FAR[4:5])
@@ -423,11 +433,7 @@
     for off in OTHERS:
         weights.block(off)
     weights.finish()
-    blocks = pl.ds(0, FS - 1)
-    sent(ball.at[pl.ds(0, len(NEAR + ACROSS)), pl.ds(0, SLICE), :], bsend)
-    sent(ball.at[pl.ds(0, len(DIAGONAL + FAR)), pl.ds(0, SLICE), :], bsend)
-    sent(ball.at[blocks, pl.ds(0, 3 * SLICE), :], ysend)
-    sent(ball.at[blocks, pl.ds(0, SIDE * SLICE), :], psems)
+    by_core(all_sent)
     sent(psend.at[peers], rsend)
     sent(pall.at[peers], asend)
     sent(sqf.at[peers], fsend)

time: 53.4 us -> 53.3 us (level)
  no operation moved by 1% of the time
where the time goes in v1:
time: 53.3 us; the launch traced here: 53 us
  Pallas kernels  52.3 us (98%)
  between operations  0.66 us (1%)
    pallas_call x1, Pallas kernels, local(): pl.pallas_call(gather_kernel, out_shape=[pltpu.VMEM(s, t) for s, t in mid...  48.8 us
    pallas_call x1, Pallas kernels, local(): pl.pallas_call(finish_kernel, out_shape=[jax.ShapeDtypeStruct(s, t) for s...  3.48 us

profile of v1, /device:TPU:0, one launch (start us, length us, event | category | flops | bytes accessed | tf_op | source)
XLA Modules:
  0.0 53.0 jit_solution(6571759172209098321)
XLA Ops:
  0.7 48.8 %gather_and_reduce.1 = (bf16[16,384,512]{2,1,0:T(8,128)(2,1)S(1)}, bf16[16,320,256]{2,1,0:T(8,128)(2,1)S(1)}, bf16[128,1024]{1,0:T(8,128)(2,1)S(1)}, f32[256,256...) custom-call(bf16[1024,4096]{1,0:T(8,128)(2,1)} %x_h.1, ...), custom_call_target="tpu_custom_call" | custom-call | tf_op jit(solution)/shard_map/gather_and_reduce/pallas_call | solution.py:493
  49.5 3.5 %write_copies.1 = (f32[256,256]{1,0:T(8,128)}, f32[256,256]{1,0:T(8,128)}, f32[128,512]{1,0:T(8,128)}, bf16[4096,256]{1,0:T(8,128)(2,1)}, bf16[4096,256]{1,0:T(8...) custom-call(bf16[16,384,512]{2,1,0:T(8,128)(2,1)S(1)} %get-tuple-ele, ...), custom_call_target="tpu_custom_call" | custom-call | tf_op jit(solution)/shard_map/write_copies/pallas_call | solution.py:530

commit v2 on v1

--- a/solution.py
+++ b/solution.py
@@ -138,6 +138,12 @@
     def blk(dz, dx):
         return lax.rem(z + (dz % SIDE), SIDE) * SIDE + lax.rem(xx + (dx % SIDE), SIDE)
 
+    barrier = pltpu.get_barrier_semaphore()
+    for off in NEAR + ACROSS:
+        pl.semaphore_signal(barrier, inc=1, device_id={"fs": blk(*off)}, device_id_type=MESH)
+    for peer in (lax.rem(t + 2, TP), lax.rem(t + TP - 2, TP), t + 1 - 2 * core):
+        pl.semaphore_signal(barrier, inc=1, device_id={"tp": peer}, device_id_type=MESH)
+
     def load(src, dst, sem):
         pltpu.make_async_copy(src, dst, lsem.at[sem]).start()
 
@@ -161,15 +167,8 @@
         load(mean_in, mean.at[:, cols], 8)
         load(square_in, square.at[:, cols], 9)
 
-    barrier = pltpu.get_barrier_semaphore()
-    for off in OTHERS:
-        pl.semaphore_signal(barrier, inc=1, device_id={"fs": blk(*off)}, device_id_type=MESH)
-    for r in range(1, TP):
-        pl.semaphore_signal(
-            barrier, inc=1, device_id={"tp": lax.rem(t + r, TP)}, device_id_type=MESH
-        )
     loaded(ball.at[f], 0)
-    pl.semaphore_wait(barrier, FS - 1 + TP - 1)
+    pl.semaphore_wait(barrier, len(NEAR + ACROSS) + 3)
 
     neighbour = [blk(0, 1), blk(0, -1), blk(1, 0), blk(-1, 0)]
     weights = Torus(wall, W_CUTS, wsend, wrecv, blk, neighbour)

time: 53.3 us -> 52.1 us (0.977)
  Pallas kernels: 52.3 us -> 51.3 us
    pallas_call x1, Pallas kernels: 48.8 us -> 47.8 us  [local(): pl.pallas_call(gather_kernel, out_shape=[pltpu.VMEM(s, t) for s, t in mid...]
where the time goes in v2:
time: 52.1 us; the launch traced here: 52 us
  Pallas kernels  51.3 us (98%)
  between operations  0.66 us (1%)
    pallas_call x1, Pallas kernels, local(): pl.pallas_call(gather_kernel, out_shape=[pltpu.VMEM(s, t) for s, t in mid...  47.8 us
    pallas_call x1, Pallas kernels, local(): pl.pallas_call(finish_kernel, out_shape=[jax.ShapeDtypeStruct(s, t) for s...  3.48 us

profile of v2, /device:TPU:0, one launch (start us, length us, event | category | flops | bytes accessed | tf_op | source)
XLA Modules:
  0.0 52.0 jit_solution(5210719692219949983)
XLA Ops:
  0.7 47.8 %gather_and_reduce.1 = (bf16[16,384,512]{2,1,0:T(8,128)(2,1)S(1)}, bf16[16,320,256]{2,1,0:T(8,128)(2,1)S(1)}, bf16[128,1024]{1,0:T(8,128)(2,1)S(1)}, f32[256,256...) custom-call(bf16[1024,4096]{1,0:T(8,128)(2,1)} %x_h.1, ...), custom_call_target="tpu_custom_call" | custom-call | tf_op jit(solution)/shard_map/gather_and_reduce/pallas_call | solution.py:492
  48.5 3.5 %write_copies.1 = (f32[256,256]{1,0:T(8,128)}, f32[256,256]{1,0:T(8,128)}, f32[128,512]{1,0:T(8,128)}, bf16[4096,256]{1,0:T(8,128)(2,1)}, bf16[4096,256]{1,0:T(8...) custom-call(bf16[16,384,512]{2,1,0:T(8,128)(2,1)S(1)} %get-tuple-ele, ...), custom_call_target="tpu_custom_call" | custom-call | tf_op jit(solution)/shard_map/write_copies/pallas_call | solution.py:529

commit v3 on v2

--- a/solution.py
+++ b/solution.py
@@ -128,7 +128,7 @@
     x, c, gq, gv, go, wqv, wo, mean, square,
     xb, cb, gt, hl, psend, precv, pall, gram, turned, d, sqf, sqs,
     lsem, wsend, wrecv, bsend, brecv, psems, psemr, ysend, yrecv, rsend, rrecv, asend, arecv,
-    fsend, frecv, ssend, srecv,
+    fsend, frecv, ssend, srecv, entered,
 ):
     f = lax.axis_index("fs")
     t = lax.axis_index("tp")
@@ -139,10 +139,15 @@
         return lax.rem(z + (dz % SIDE), SIDE) * SIDE + lax.rem(xx + (dx % SIDE), SIDE)
 
     barrier = pltpu.get_barrier_semaphore()
-    for off in NEAR + ACROSS:
+    for off in ACROSS + NEAR:
         pl.semaphore_signal(barrier, inc=1, device_id={"fs": blk(*off)}, device_id_type=MESH)
-    for peer in (lax.rem(t + 2, TP), lax.rem(t + TP - 2, TP), t + 1 - 2 * core):
+    for peer in (lax.rem(t + 2, TP), lax.rem(t + TP - 2, TP)):
         pl.semaphore_signal(barrier, inc=1, device_id={"tp": peer}, device_id_type=MESH)
+
+    @pl.when(core == 0)
+    def _():
+        pl.semaphore_signal(barrier, inc=1, device_id={"tp": t + 1}, device_id_type=MESH)
+
 
     def load(src, dst, sem):
         pltpu.make_async_copy(src, dst, lsem.at[sem]).start()
@@ -168,7 +173,12 @@
         load(square_in, square.at[:, cols], 9)
 
     loaded(ball.at[f], 0)
-    pl.semaphore_wait(barrier, len(NEAR + ACROSS) + 3)
+    pl.semaphore_wait(barrier, len(NEAR + ACROSS) + 2 + core)
+
+    @pl.when(core == 1)
+    def _():
+        pl.semaphore_signal(entered, inc=1, device_id={"tp": t - 1}, device_id_type=MESH)
+
 
     neighbour = [blk(0, 1), blk(0, -1), blk(1, 0), blk(-1, 0)]
     weights = Torus(wall, W_CUTS, wsend, wrecv, blk, neighbour)
@@ -292,10 +302,14 @@
     by_core(functools.partial(relay_levels, 1))
     by_core(functools.partial(send_levels, 3))
     weights.step(4)
+    @pl.when(core == 0)
+    def _():
+        pl.semaphore_wait(entered, 1)
+
     by_core(functools.partial(hand_over, 0))
     by_core(functools.partial(relay_levels, 2))
+    weights.step(5)
     by_core(functools.partial(hand_over, 1))
-    weights.step(5)
     by_core(functools.partial(relay_levels, 3))
     weights.step(6)
     by_core(functools.partial(handed, 0))
@@ -519,6 +533,7 @@
             dma((10,)),
             dma, dma((STEPS,)), dma, dma((4,)), dma, dma((4,)), dma, dma((8,)),
             dma, dma, dma, dma((2,)), dma, dma, dma, dma,
+            pltpu.SemaphoreType.REGULAR,
         ],
         compiler_params=pltpu.CompilerParams(
             collective_id=0, has_side_effects=True, vmem_limit_bytes=50 * 1024 * 1024

time: 52.1 us -> 52.1 us (level)
  no operation moved by 1% of the time
where the time goes in v3:
time: 52.1 us; the launch traced here: 52 us
  Pallas kernels  51.3 us (98%)
  between operations  0.66 us (1%)
    pallas_call x1, Pallas kernels, local(): pl.pallas_call(gather_kernel, out_shape=[pltpu.VMEM(s, t) for s, t in mid...  47.9 us
    pallas_call x1, Pallas kernels, local(): pl.pallas_call(finish_kernel, out_shape=[jax.ShapeDtypeStruct(s, t) for s...  3.48 us

profile of v3, /device:TPU:0, one launch (start us, length us, event | category | flops | bytes accessed | tf_op | source)
XLA Modules:
  0.0 52.0 jit_solution(7024568070469637118)
XLA Ops:
  0.7 47.9 %gather_and_reduce.1 = (bf16[16,384,512]{2,1,0:T(8,128)(2,1)S(1)}, bf16[16,320,256]{2,1,0:T(8,128)(2,1)S(1)}, bf16[128,1024]{1,0:T(8,128)(2,1)S(1)}, f32[256,256...) custom-call(bf16[1024,4096]{1,0:T(8,128)(2,1)} %x_h.1, ...), custom_call_target="tpu_custom_call" | custom-call | tf_op jit(solution)/shard_map/gather_and_reduce/pallas_call | solution.py:506
  48.5 3.5 %write_copies.1 = (f32[256,256]{1,0:T(8,128)}, f32[256,256]{1,0:T(8,128)}, f32[128,512]{1,0:T(8,128)}, bf16[4096,256]{1,0:T(8,128)(2,1)}, bf16[4096,256]{1,0:T(8...) custom-call(bf16[16,384,512]{2,1,0:T(8,128)(2,1)S(1)} %get-tuple-ele, ...), custom_call_target="tpu_custom_call" | custom-call | tf_op jit(solution)/shard_map/write_copies/pallas_call | solution.py:544
